TPU v7x, 32 devices: a whole 2x2x4 slice. The times are simulated.
32 devices in a mesh: sp: 8 (over z, y), tp: 4 (over x, core).
Axes of the slice: x: 2, y: 2, z: 4, core: 2. Of those that a mesh axis runs over, the one named last changes fastest.
Arguments:
- tokens: bfloat16 [4096, 2048], P(('sp', 'tp')), may hold values from -6 to 6
- queries: bfloat16 [4096, 1024], P('sp', 'tp'), may hold values from -160 to 160
- keys: bfloat16 [4096, 1024], P('sp', 'tp'), may hold values from -8 to 8
- values: bfloat16 [4096, 1024], P('sp', 'tp'), may hold values from -6 to 6
- lambdas: float32 [8], P('tp'), may hold values from 0.3 to 0.8
- head_gain: float32 [128], replicated, may hold values from 0.1 to 1.9
- out_weight: bfloat16 [1024, 2048], replicated, may hold values from -0.1875 to 0.1875
- mixer_gain: float32 [2048], replicated, may hold values from 0.1 to 1.9
- up_weight: bfloat16 [2048, 4096], P('sp', 'tp'), may hold values from -0.125 to 0.125
- down_weight: bfloat16 [4096, 2048], P('tp', 'sp'), may hold values from -0.09375 to 0.09375
Outputs:
- result: bfloat16 [4096, 2048], P(('sp', 'tp'))
All inputs are finite; a program needn't handle non-finite values.
Results may differ from a plain program's by a relative error of at most 0.02.
Values may be sent and summed in bfloat16 or wider, within the bound.
A program may use at most 128 MiB of HBM per device.

v0:
```python
import math
import jax
import jax.numpy as jnp
from jax import lax
from jax.sharding import PartitionSpec as P

DQK = 64
DV = 128


def per_device(
    tokens,
    queries,
    keys,
    values,
    lambdas,
    head_gain,
    out_weight,
    mixer_gain,
    up_weight,
    down_weight,
):
    tok_rows = queries.shape[0]
    head_count = lambdas.shape[0]
    scaling = DQK ** (-0.5)
    sp_index = lax.axis_index("sp")
    first_row = sp_index * tok_rows
    last_row = first_row + tok_rows - 1
    query_split = queries.reshape(tok_rows, head_count, 2, DQK)
    query_pos = first_row + lax.broadcasted_iota(jnp.int32, (tok_rows, 1), 0)
    floor_max = jnp.full((head_count, tok_rows), -1e30, jnp.float32)
    zero_total = jnp.zeros((head_count, tok_rows), jnp.float32)
    zero_acc = jnp.zeros((head_count, tok_rows, DV), jnp.float32)
    start_state = (floor_max, zero_total, zero_acc, floor_max, zero_total, zero_acc)
    key_piece = lax.all_gather(keys, "sp", axis=0, tiled=True)
    value_piece = lax.all_gather(values, "sp", axis=0, tiled=True)
    piece_rows = key_piece.shape[0]
    block_width = math.gcd(piece_rows, 512)

    def one_block(block_index, running):
        offset = block_index * block_width

        def update(inner):
            key_block = lax.dynamic_slice_in_dim(key_piece, offset, block_width, 0).reshape(
                block_width, head_count, 2, DQK
            )
            value_block = lax.dynamic_slice_in_dim(value_piece, offset, block_width, 0).reshape(
                block_width, head_count, DV
            )
            key_pos = offset + lax.broadcasted_iota(jnp.int32, (1, block_width), 1)
            allowed = key_pos <= query_pos
            updated = []
            for map_index in range(2):
                run_max = inner[3 * map_index]
                run_total = inner[3 * map_index + 1]
                run_acc = inner[3 * map_index + 2]
                scores = (
                    jnp.einsum(
                        "qhd,khd->hqk",
                        query_split[:, :, map_index],
                        key_block[:, :, map_index],
                        preferred_element_type=jnp.float32,
                    )
                    * scaling
                )
                scores = jnp.where(allowed[None], scores, -jnp.inf)
                new_max = jnp.maximum(run_max, jnp.max(scores, axis=2))
                shrink = jnp.exp(run_max - new_max)
                exponent = jnp.exp(scores - new_max[:, :, None])
                new_total = run_total * shrink + jnp.sum(exponent, axis=2)
                new_acc = run_acc * shrink[:, :, None] + jnp.einsum(
                    "hqk,khd->hqd",
                    exponent.astype(jnp.bfloat16),
                    value_block,
                    preferred_element_type=jnp.float32,
                )
                updated += [new_max, new_total, new_acc]
            return tuple(updated)

        return lax.cond(offset <= last_row, update, lambda inner: inner, running)

    final = lax.fori_loop(0, piece_rows // block_width, one_block, start_state)
    first_map = final[2] / final[1][:, :, None]
    second_map = final[5] / final[4][:, :, None]
    differ = first_map - lambdas[:, None, None] * second_map
    spread = lax.rsqrt(jnp.mean(differ * differ, axis=2, keepdims=True) + 1e-06)
    attended = (differ * spread * head_gain).astype(jnp.bfloat16)
    attended = jnp.transpose(attended, (1, 0, 2)).reshape(tok_rows, head_count * DV)
    all_heads = lax.all_to_all(attended, "tp", split_axis=0, concat_axis=1, tiled=True)
    projected = jnp.dot(all_heads, out_weight, preferred_element_type=jnp.float32).astype(
        jnp.bfloat16
    )
    resid = (tokens.astype(jnp.float32) + projected.astype(jnp.float32)).astype(jnp.bfloat16)
    resid_full = resid.astype(jnp.float32)
    normed = (
        resid_full
        * lax.rsqrt(jnp.mean(resid_full * resid_full, axis=1, keepdims=True) + 1e-06)
        * mixer_gain
    ).astype(jnp.bfloat16)
    up_full, down_full = (
        lax.all_gather(up_weight, "sp", axis=0, tiled=True),
        lax.all_gather(down_weight, "sp", axis=1, tiled=True),
    )
    hidden = jnp.square(
        jax.nn.relu(
            jnp.dot(
                lax.all_gather(normed, "tp", axis=0, tiled=True),
                up_full,
                preferred_element_type=jnp.float32,
            )
        )
    ).astype(jnp.bfloat16)
    mixed = lax.psum_scatter(
        jnp.dot(hidden, down_full, preferred_element_type=jnp.float32).astype(jnp.bfloat16),
        "tp",
        scatter_dimension=0,
        tiled=True,
    ).astype(jnp.float32)
    return (resid_full + mixed).astype(jnp.bfloat16)


def solution(mesh):
    placed = (
        P(("sp", "tp"), None),
        P("sp", "tp"),
        P("sp", "tp"),
        P("sp", "tp"),
        P("tp"),
        P(),
        P(),
        P(),
        P("sp", "tp"),
        P("tp", "sp"),
    )
    return jax.shard_map(
        per_device, mesh=mesh, in_specs=placed, out_specs=P(("sp", "tp"), None), check_vma=False
    )
```

profile of v0, /device:TPU:0, one launch (start us, length us, event | category | flops | bytes accessed | tf_op | source)
XLA Modules:
  0.0 390.4 jit_solution(7003081648482967234)
XLA Ops:
  6.5 1.8 copy.19
  8.4 1.8 copy.21
  10.3 1.1 copy.20
  11.4 51.1 %all-gather.6.cloned.1.call-done = bf16[4096,256]{0,1:T(8,128)(2,1)} async-done(((bf16[512,256]{0,1:T(8,128)(2,1)}), bf16[4096,256]{0,1:T(8,128)(2,1)}) %all-gather.6.cloned.1.call-update) | async-done | bytes 2097168 | tf_op jit(solution)/shard_map/all_gather | solution.py:35
  62.5 50.6 %all-gather.8.cloned.1.call-done = bf16[4096,256]{0,1:T(8,128)(2,1)} async-done(((bf16[512,256]{0,1:T(8,128)(2,1)}), bf16[4096,256]{0,1:T(8,128)(2,1)}) %all-gather.8.cloned.1.call-update) | async-done | bytes 2097168 | tf_op jit(solution)/shard_map/all_gather | solution.py:36
  113.2 6.1 %while.24 = (s32[]{:T(128)}, f32[2,512]{1,0:T(2,128)S(1)}, f32[2,512]{1,0:T(2,128)S(1)}, f32[2,512,128]{2,1,0:T(8,128)S(1)}, f32[2,512]{1,0:T(2,128)S(1)}, /*ind...) while((s32[]{:T(128)}, f32[2,512]{1,0:T(2,128)S(1)}, ...), condition=%wide.region_7.8_spmd.clone, body=%wide.region_0.7_spmd.clone.sunk | while | flops 410784768 | bytes 17707416 | solution.py:82
  113.3 5.6 %conditional.3 = ((f32[2,512]{1,0:T(2,128)S(1)}, f32[2,512]{1,0:T(2,128)S(1)}, f32[2,512,128]{2,1,0:T(8,128)S(1)}, f32[2,512]{1,0:T(2,128)S(1)}, f32[2,512]{1,0:T(2,128)S(1)}, /*index=5*/f32[2,512,128]{2,1,0:T(8,128)S(1)})) conditional(s32[]{:T(128)} %convert_element_type.94, (f32[2,512]{1,0:T(2,128)S(1)}, f32[2,512]{1,0:T(2,128)S(1)}, ...), branch_computations={%region_1.0_spmd, %region_2.6_spmd} | conditional | flops 410784768 | bytes 17705066 | solution.py:80
  113.3 1.0 constant_dynamic-slice_fusion.1
  114.5 0.6 fusion.20
  115.5 0.6 fusion.21
  116.4 1.0 constant_dynamic-slice_fusion
  117.4 0.7 convolution_add_fusion
  118.1 0.7 convolution_add_fusion.1
  120.5 8.5 %all_to_all.19 = bf16[4,128,256]{2,1,0:T(8,128)(2,1)S(1)} all-to-all(bf16[4,128,256]{2,1,0:T(8,128)(2,1)S(1)} %all_to_all.14), channel_id=1, replica_groups=mesh['sp'=8,'tp'=4] {'tp'}, dimensions={0} | all-to-all | bytes 524288 | tf_op jit(solution)/shard_map/all_to_all | solution.py:89
  129.3 3.0 multiply_reduce_fusion
  132.3 1.0 multiply_convert_fusion.1
  133.3 0.5 all-gather.12.cloned.1.call-update
  133.9 0.5 all-gather.14.cloned.1.call-update
  134.5 57.8 %all-gather.10.cloned.1.call-done = bf16[512,2048]{1,0:T(8,128)(2,1)} async-done(((bf16[128,2048]{1,0:T(8,128)(2,1)}), bf16[512,2048]{1,0:T(8,128)(2,1)}) %all-gather.10.cloned.1.call-update) | async-done | bytes 2097168 | tf_op jit(solution)/shard_map/all_gather | solution.py:107
  192.3 74.8 %all-gather.12.cloned.1.call-done = bf16[2048,1024]{1,0:T(8,128)(2,1)} async-done(((bf16[256,1024]{1,0:T(8,128)(2,1)}), bf16[2048,1024]{1,0:T(8,128)(2,1)}) %all-gather.12.cloned.1.call-update) | async-done | bytes 4194320 | tf_op jit(solution)/shard_map/all_gather | solution.py:101
  267.1 75.1 %all-gather.14.cloned.1.call-done = bf16[1024,2048]{1,0:T(8,128)(2,1)} async-done(((bf16[1024,256]{1,0:T(8,128)(2,1)}), bf16[1024,2048]{1,0:T(8,128)(2,1)}) %all-gather.14.cloned.1.call-update) | async-done | bytes 4194320 | tf_op jit(solution)/shard_map/all_gather | solution.py:102
  342.2 9.9 %convolution_convert_fusion = bf16[512,2048]{1,0:T(8,128)(2,1)} fusion(bf16[1024,2048]{1,0:T(8,128)(2,1)} %all-gather.14.cloned.1.call-done, bf16[512,2048]{1,0:T(8,128)(2,1)} %all-gather.10.cloned.1.call-done, bf16[2048,1024]{1,0:T(8,128)(2,1)} %all-gather.12.cloned.1.call-done), kind=kOutput, calls=%fused_computation.28 | convolution fusion | flops 4297588736 | bytes 12582912 | tf_op jit(solution)/shard_map/dot_general | solution.py:114
  352.1 29.5 %reduce-scatter.2.cloned.1.call-done = bf16[128,2048]{1,0:T(8,128)(2,1)} async-done(((bf16[512,2048]{1,0:T(8,128)(2,1)}), bf16[128,2048]{1,0:T(8,128)(2,1)}) %reduce-scatter.2.cloned.1.call-update) | async-done | bytes 524304 | tf_op jit(solution)/shard_map/reduce_scatter | solution.py:113
  381.6 1.9 add_convert_fusion
  (57 shorter events, 2.8 us)
Async XLA Ops:
  6.5 55.9 %all-gather.6.cloned.1.call-start = ((), (), s32[]{:S(2)}) async-start(), calls=%async_computation.2 | async-start | bytes 2359296 | tf_op jit(solution)/shard_map/all_gather | solution.py:35
  8.4 104.7 %all-gather.8.cloned.1.call-start = ((), (), s32[]{:S(2)}) async-start(), calls=%async_computation.3 | async-start | bytes 2359296 | tf_op jit(solution)/shard_map/all_gather | solution.py:36
  10.2 182.1 %all-gather.10.cloned.1.call-start = ((), (), s32[]{:S(2)}) async-start(), calls=%async_computation.4 | async-start | bytes 2621440 | tf_op jit(solution)/shard_map/all_gather | solution.py:107
  113.2 6.1 %copy-start.2 = (f32[2]{0:T(128)S(1)}, f32[2]{0:T(128)}, u32[]{:S(2)}) copy-start(f32[2]{0:T(128)} %param.18) | copy-start | bytes 28
  113.2 6.6 %copy-start.3 = (f32[128]{0:T(128)S(1)}, f32[128]{0:T(128)}, u32[]{:S(2)}) copy-start(f32[128]{0:T(128)} %param.19) | copy-start | bytes 1540
  119.3 9.9 %copy-start = (bf16[128,2048]{1,0:T(8,128)(2,1)S(1)}, bf16[128,2048]{1,0:T(8,128)(2,1)}, u32[]{:S(2)}) copy-start(bf16[128,2048]{1,0:T(8,128)(2,1)} %param.14) | copy-start | bytes 1572868
  129.3 3.0 copy-start.1
  133.3 133.8 %all-gather.12.cloned.1.call-start = ((), (), s32[]{:S(2)}) async-start(), calls=%async_computation.5 | async-start | bytes 4718592 | tf_op jit(solution)/shard_map/all_gather | solution.py:101
  133.9 208.3 %all-gather.14.cloned.1.call-start = ((), (), s32[]{:S(2)}) async-start(), calls=%async_computation.6 | async-start | bytes 4718592 | tf_op jit(solution)/shard_map/all_gather | solution.py:102
  134.5 247.2 %reduce-scatter.2.cloned.1.call-start = ((), (), s32[]{:S(2)}) async-start(), calls=%async_computation.7 | async-start | bytes 2621440 | tf_op jit(solution)/shard_map/reduce_scatter | solution.py:113
Sparse Core Ops, SparseCore 0:
  9.4 53.0 all-gather.5
  64.5 48.5 all-gather.7
  133.4 58.8 all-gather.9
  194.3 72.7 all-gather.11
  269.0 73.1 all-gather.13
  352.3 29.3 reduce-scatter.1
where the time goes:
time: 391 us; the launch traced here: 390 us
  waiting for transfers between devices  340 us (87%)
  matrix products  15.6 us (4%)
  between operations  13.6 us (3%)
  blocking collectives  8.55 us (2%)
  local copies, waits for them, and re-layouts  7.41 us (2%)
  other arithmetic  4.49 us (1%)
    all_gather x1, waiting for transfers between devices, per_device(): lax.all_gather(down_weight, 'sp', axis=1, tiled=True)  75.1 us
    all_gather x1, waiting for transfers between devices, per_device(): lax.all_gather(up_weight, 'sp', axis=0, tiled=True)  74.8 us
    all_gather x1, waiting for transfers between devices, per_device(): lax.all_gather(normed, 'tp', axis=0, tiled=True)  57.8 us
    all_gather x1, waiting for transfers between devices, per_device(): key_piece = lax.all_gather(keys, 'sp', axis=0, tiled=True)  51.1 us
    all_gather x1, waiting for transfers between devices, per_device(): value_piece = lax.all_gather(values, 'sp', axis=0, tiled=True)  50.6 us
    reduce_scatter x1, waiting for transfers between devices, per_device(): lax.psum_scatter(jnp.dot(hidden, down_full, preferred_element_type=jnp.fl...  29.5 us
    dot_general x1, matrix products, per_device(): jnp.dot(hidden, down_full, preferred_element_type=jnp.float32)  9.93 us
    all_to_all x1, blocking collectives, per_device(): lax.all_to_all(attended, 'tp', split_axis=0, concat_axis=1, tiled=True)  8.55 us
  transfers between devices with their start and end apart: 6, of which 6 were waited for; matrix products, arithmetic and copies ran while one was open for 1% of the time, Pallas kernels for 0%

commit v1 on v0

--- a/solution.py
+++ b/solution.py
@@ -32,7 +32,12 @@
     zero_total = jnp.zeros((head_count, tok_rows), jnp.float32)
     zero_acc = jnp.zeros((head_count, tok_rows, DV), jnp.float32)
     start_state = (floor_max, zero_total, zero_acc, floor_max, zero_total, zero_acc)
-    key_piece = lax.all_gather(keys, "sp", axis=0, tiled=True)
+    ring = [keys]
+    for hop in range(7):
+        ring.append(lax.ppermute(ring[-1], "sp", [(dev, (dev + 1) % 8) for dev in range(8)]))
+    key_piece = jnp.roll(
+        jnp.concatenate(ring[::-1], axis=0), (lax.axis_index("sp") + 1) * ring[0].shape[0], axis=0
+    )
     value_piece = lax.all_gather(values, "sp", axis=0, tiled=True)
     piece_rows = key_piece.shape[0]
     block_width = math.gcd(piece_rows, 512)

time: 391 us -> 365 us (0.934)
  waiting for transfers between devices: 340 us -> 311 us
    ppermute x0 -> x7, waiting for transfers between devices: none -> 78.5 us  [per_device(): lax.ppermute(ring[-1], 'sp', [(dev, (dev + 1) % 8) for dev in range(8)])]
    all_gather x1 -> x0, waiting for transfers between devices: 51.1 us -> none  [per_device(): key_piece = lax.all_gather(keys, 'sp', axis=0, tiled=True)]
    all_gather x1, waiting for transfers between devices: 50.6 us -> 1.34 us  [per_device(): value_piece = lax.all_gather(values, 'sp', axis=0, tiled=True)]
    all_gather x1, waiting for transfers between devices: 57.8 us -> 50.6 us  [per_device(): lax.all_gather(normed, 'tp', axis=0, tiled=True)]
  transfers between devices with their start and end apart: 6 -> 12, of which waited for: 6 -> 12; matrix products, arithmetic and copies ran while one was open for 1% -> 1% of each run, Pallas kernels for 0% -> 0%
where the time goes in v1:
time: 365 us; the launch traced here: 364 us
  waiting for transfers between devices  311 us (85%)
  matrix products  15.6 us (4%)
  between operations  13.5 us (4%)
  blocking collectives  9.58 us (3%)
  local copies, waits for them, and re-layouts  6.36 us (2%)
  other arithmetic  4.49 us (1%)
    ppermute x7, waiting for transfers between devices, per_device(): lax.ppermute(ring[-1], 'sp', [(dev, (dev + 1) % 8) for dev in range(8)])  78.5 us
    all_gather x1, waiting for transfers between devices, per_device(): lax.all_gather(down_weight, 'sp', axis=1, tiled=True)  76.7 us
    all_gather x1, waiting for transfers between devices, per_device(): lax.all_gather(up_weight, 'sp', axis=0, tiled=True)  73 us
    all_gather x1, waiting for transfers between devices, per_device(): lax.all_gather(normed, 'tp', axis=0, tiled=True)  50.6 us
    reduce_scatter x1, waiting for transfers between devices, per_device(): lax.psum_scatter(jnp.dot(hidden, down_full, preferred_element_type=jnp.fl...  29.8 us
    dot_general x1, matrix products, per_device(): jnp.dot(hidden, down_full, preferred_element_type=jnp.float32)  9.94 us
    all_to_all x1, blocking collectives, per_device(): lax.all_to_all(attended, 'tp', split_axis=0, concat_axis=1, tiled=True)  9.58 us
  transfers between devices with their start and end apart: 12, of which 12 were waited for; matrix products, arithmetic and copies ran while one was open for 1% of the time, Pallas kernels for 0%

profile of v1, /device:TPU:0, one launch (start us, length us, event | category | flops | bytes accessed | tf_op | source)
XLA Modules:
  0.0 364.5 jit_solution(16382751065413296117)
XLA Ops:
  6.5 1.1 copy.19
  7.6 3.0 collective-permute-start
  10.7 9.3 %collective-permute-done = bf16[512,256]{0,1:T(8,128)(2,1)S(1)} collective-permute-done((bf16[512,256]{0,1:T(8,128)(2,1)S(1)}, bf16[512,256]{0,1:T(8,128)(2,1)S(1)}, u32[]{:S(2)}, u32[]{:S(2)}) %collective-permute-start) | collective-permute-done | bytes 262176 | tf_op jit(solution)/shard_map/ppermute | solution.py:37
  20.0 10.2 %collective-permute-done.1 = bf16[512,256]{0,1:T(8,128)(2,1)S(1)} collective-permute-done((bf16[512,256]{0,1:T(8,128)(2,1)S(1)}, bf16[512,256]{0,1:T(8,128)(2,1)S(1)}, u32[]{:S(2)}, u32[]{:S(2)}) %collective-permute-start.1) | collective-permute-done | bytes 262176 | tf_op jit(solution)/shard_map/ppermute | solution.py:37
  30.2 1.8 copy.23
  32.1 7.4 %collective-permute-done.2 = bf16[512,256]{0,1:T(8,128)(2,1)S(1)} collective-permute-done((bf16[512,256]{0,1:T(8,128)(2,1)S(1)}, bf16[512,256]{0,1:T(8,128)(2,1)S(1)}, u32[]{:S(2)}, u32[]{:S(2)}) %collective-permute-start.2) | collective-permute-done | bytes 262176 | tf_op jit(solution)/shard_map/ppermute | solution.py:37
  39.5 12.4 %collective-permute-done.3 = bf16[512,256]{0,1:T(8,128)(2,1)S(1)} collective-permute-done((bf16[512,256]{0,1:T(8,128)(2,1)S(1)}, bf16[512,256]{0,1:T(8,128)(2,1)S(1)}, u32[]{:S(2)}, u32[]{:S(2)}) %collective-permute-start.3) | collective-permute-done | bytes 262176 | tf_op jit(solution)/shard_map/ppermute | solution.py:37
  51.9 12.0 %collective-permute-done.4 = bf16[512,256]{0,1:T(8,128)(2,1)S(1)} collective-permute-done((bf16[512,256]{0,1:T(8,128)(2,1)S(1)}, bf16[512,256]{0,1:T(8,128)(2,1)S(1)}, u32[]{:S(2)}, u32[]{:S(2)}) %collective-permute-start.4) | collective-permute-done | bytes 262176 | tf_op jit(solution)/shard_map/ppermute | solution.py:37
  63.9 13.5 %collective-permute-done.5 = bf16[512,256]{0,1:T(8,128)(2,1)S(1)} collective-permute-done((bf16[512,256]{0,1:T(8,128)(2,1)S(1)}, bf16[512,256]{0,1:T(8,128)(2,1)S(1)}, u32[]{:S(2)}, u32[]{:S(2)}) %collective-permute-start.5) | collective-permute-done | bytes 262176 | tf_op jit(solution)/shard_map/ppermute | solution.py:37
  77.4 1.1 copy.22
  78.5 13.7 %collective-permute-done.6 = bf16[512,256]{0,1:T(8,128)(2,1)S(1)} collective-permute-done((bf16[512,256]{0,1:T(8,128)(2,1)S(1)}, bf16[512,256]{0,1:T(8,128)(2,1)S(1)}, u32[]{:S(2)}, u32[]{:S(2)}) %collective-permute-start.6) | collective-permute-done | bytes 262176 | tf_op jit(solution)/shard_map/ppermute | solution.py:37
  92.9 1.3 all-gather.5.cloned.1.call-done
  94.4 5.1 %while.24 = (s32[]{:T(128)}, f32[2,512]{1,0:T(2,128)S(1)}, f32[2,512]{1,0:T(2,128)S(1)}, f32[2,512,128]{2,1,0:T(8,128)S(1)}, f32[2,512]{1,0:T(2,128)S(1)}, /*ind...) while((s32[]{:T(128)}, f32[2,512]{1,0:T(2,128)S(1)}, ...), condition=%wide.region_7.8_spmd.clone, body=%wide.region_0.7_spmd.clone.sunk | while | flops 410784768 | bytes 17707416 | solution.py:87
  94.5 4.7 %conditional.3 = ((f32[2,512]{1,0:T(2,128)S(1)}, f32[2,512]{1,0:T(2,128)S(1)}, f32[2,512,128]{2,1,0:T(8,128)S(1)}, f32[2,512]{1,0:T(2,128)S(1)}, f32[2,512]{1,0:T(2,128)S(1)}, /*index=5*/f32[2,512,128]{2,1,0:T(8,128)S(1)})) conditional(s32[]{:T(128)} %convert_element_type.94, (f32[2,512]{1,0:T(2,128)S(1)}, f32[2,512]{1,0:T(2,128)S(1)}, ...), branch_computations={%region_1.1_spmd, %region_2.6_spmd} | conditional | flops 410784768 | bytes 17705066 | solution.py:85
  96.7 1.0 constant_dynamic-slice_fusion
  100.8 9.6 %all_to_all.19 = bf16[4,128,256]{2,1,0:T(8,128)(2,1)S(1)} all-to-all(bf16[4,128,256]{2,1,0:T(8,128)(2,1)S(1)} %all_to_all.14), channel_id=1, replica_groups=mesh['sp'=8,'tp'=4] {'tp'}, dimensions={0} | all-to-all | bytes 524288 | tf_op jit(solution)/shard_map/all_to_all | solution.py:94
  110.6 3.0 multiply_reduce_fusion
  113.6 1.0 multiply_convert_fusion.1
  115.9 50.6 %all-gather.7.cloned.1.call-done = bf16[512,2048]{1,0:T(8,128)(2,1)} async-done(((bf16[128,2048]{1,0:T(8,128)(2,1)}), bf16[512,2048]{1,0:T(8,128)(2,1)}) %all-gather.7.cloned.1.call-update) | async-done | bytes 2097168 | tf_op jit(solution)/shard_map/all_gather | solution.py:112
  166.5 76.7 %all-gather.11.cloned.1.call-done = bf16[1024,2048]{1,0:T(8,128)(2,1)} async-done(((bf16[1024,256]{1,0:T(8,128)(2,1)}), bf16[1024,2048]{1,0:T(8,128)(2,1)}) %all-gather.11.cloned.1.call-update) | async-done | bytes 4194320 | tf_op jit(solution)/shard_map/all_gather | solution.py:107
  243.2 73.0 %all-gather.9.cloned.1.call-done = bf16[2048,1024]{1,0:T(8,128)(2,1)} async-done(((bf16[256,1024]{1,0:T(8,128)(2,1)}), bf16[2048,1024]{1,0:T(8,128)(2,1)}) %all-gather.9.cloned.1.call-update) | async-done | bytes 4194320 | tf_op jit(solution)/shard_map/all_gather | solution.py:106
  316.2 9.9 %convolution_convert_fusion = bf16[512,2048]{1,0:T(8,128)(2,1)} fusion(bf16[1024,2048]{1,0:T(8,128)(2,1)} %all-gather.11.cloned.1.call-done, bf16[512,2048]{1,0:T(8,128)(2,1)} %all-gather.7.cloned.1.call-done, bf16[2048,1024]{1,0:T(8,128)(2,1)} %all-gather.9.cloned.1.call-done), kind=kOutput, calls=%fused_computation.28 | convolution fusion | flops 4297588736 | bytes 12582912 | tf_op jit(solution)/shard_map/dot_general | solution.py:119
  326.2 29.8 %reduce-scatter.2.cloned.1.call-done = bf16[128,2048]{1,0:T(8,128)(2,1)} async-done(((bf16[512,2048]{1,0:T(8,128)(2,1)}), bf16[128,2048]{1,0:T(8,128)(2,1)}) %reduce-scatter.2.cloned.1.call-update) | async-done | bytes 524304 | tf_op jit(solution)/shard_map/reduce_scatter | solution.py:118
  356.0 1.9 add_convert_fusion
  (85 shorter events, 7.2 us)
Async XLA Ops:
  6.5 87.7 %all-gather.5.cloned.1.call-start = ((), (), s32[]{:S(2)}) async-start(), calls=%async_computation.2 | async-start | bytes 2359296 | tf_op jit(solution)/shard_map/all_gather | solution.py:41
  7.6 12.4 %collective-permute-start = (bf16[512,256]{0,1:T(8,128)(2,1)S(1)}, bf16[512,256]{0,1:T(8,128)(2,1)S(1)}, u32[]{:S(2)}, u32[]{:S(2)}) collective-permute-start(bf16[512,256]{0,1:T(8,128)(2,1)S(1)} %copy.19), channel_id=1, source_target_pairs={{0,4},{4,8},{8,12},{12,16},{16,20},{20,24},{24,28},{28,0},{1,5},{5... | collective-permute-start | bytes 786440 | tf_op jit(solution)/shard_map/ppermute | solution.py:37
  20.0 10.2 %collective-permute-start.1 = (bf16[512,256]{0,1:T(8,128)(2,1)S(1)}, bf16[512,256]{0,1:T(8,128)(2,1)S(1)}, u32[]{:S(2)}, u32[]{:S(2)}) collective-permute-start(bf16[512,256]{0,1:T(8,128)(2,1)S(1)} %collective-permute-done), channel_id=1, source_target_pairs={{0,4},{4,8},{8,12},{12,16},{16,20},{20,24},{24,28},{28,0},{1,5},{5... | collective-permute-start | bytes 786440 | tf_op jit(solution)/shard_map/ppermute | solution.py:37
  30.2 9.3 %collective-permute-start.2 = (bf16[512,256]{0,1:T(8,128)(2,1)S(1)}, bf16[512,256]{0,1:T(8,128)(2,1)S(1)}, u32[]{:S(2)}, u32[]{:S(2)}) collective-permute-start(bf16[512,256]{0,1:T(8,128)(2,1)S(1)} %collective-permute-done.1), channel_id=1, source_target_pairs={{0,4},{4,8},{8,12},{12,16},{16,20},{20,24},{24,28},{28,0},{1,5},{5... | collective-permute-start | bytes 786440 | tf_op jit(solution)/shard_map/ppermute | solution.py:37
  32.0 134.5 %all-gather.7.cloned.1.call-start = ((), (), s32[]{:S(2)}) async-start(), calls=%async_computation.3 | async-start | bytes 2621440 | tf_op jit(solution)/shard_map/all_gather | solution.py:112
  39.5 12.4 %collective-permute-start.3 = (bf16[512,256]{0,1:T(8,128)(2,1)S(1)}, bf16[512,256]{0,1:T(8,128)(2,1)S(1)}, u32[]{:S(2)}, u32[]{:S(2)}) collective-permute-start(bf16[512,256]{0,1:T(8,128)(2,1)S(1)} %collective-permute-done.2), channel_id=1, source_target_pairs={{0,4},{4,8},{8,12},{12,16},{16,20},{20,24},{24,28},{28,0},{1,5},{5... | collective-permute-start | bytes 786440 | tf_op jit(solution)/shard_map/ppermute | solution.py:37
  51.9 12.0 %collective-permute-start.4 = (bf16[512,256]{0,1:T(8,128)(2,1)S(1)}, bf16[512,256]{0,1:T(8,128)(2,1)S(1)}, u32[]{:S(2)}, u32[]{:S(2)}) collective-permute-start(bf16[512,256]{0,1:T(8,128)(2,1)S(1)} %collective-permute-done.3), channel_id=1, source_target_pairs={{0,4},{4,8},{8,12},{12,16},{16,20},{20,24},{24,28},{28,0},{1,5},{5... | collective-permute-start | bytes 786440 | tf_op jit(solution)/shard_map/ppermute | solution.py:37
  63.9 13.5 %collective-permute-start.5 = (bf16[512,256]{0,1:T(8,128)(2,1)S(1)}, bf16[512,256]{0,1:T(8,128)(2,1)S(1)}, u32[]{:S(2)}, u32[]{:S(2)}) collective-permute-start(bf16[512,256]{0,1:T(8,128)(2,1)S(1)} %collective-permute-done.4), channel_id=1, source_target_pairs={{0,4},{4,8},{8,12},{12,16},{16,20},{20,24},{24,28},{28,0},{1,5},{5... | collective-permute-start | bytes 786440 | tf_op jit(solution)/shard_map/ppermute | solution.py:37
  77.4 14.8 %collective-permute-start.6 = (bf16[512,256]{0,1:T(8,128)(2,1)S(1)}, bf16[512,256]{0,1:T(8,128)(2,1)S(1)}, u32[]{:S(2)}, u32[]{:S(2)}) collective-permute-start(bf16[512,256]{0,1:T(8,128)(2,1)S(1)} %collective-permute-done.5), channel_id=1, source_target_pairs={{0,4},{4,8},{8,12},{12,16},{16,20},{20,24},{24,28},{28,0},{1,5},{5... | collective-permute-start | bytes 786440 | tf_op jit(solution)/shard_map/ppermute | solution.py:37
  94.4 5.2 %copy-start.2 = (f32[2]{0:T(128)S(1)}, f32[2]{0:T(128)}, u32[]{:S(2)}) copy-start(f32[2]{0:T(128)} %param.18) | copy-start | bytes 28
  94.4 5.7 %copy-start.3 = (f32[128]{0:T(128)S(1)}, f32[128]{0:T(128)}, u32[]{:S(2)}) copy-start(f32[128]{0:T(128)} %param.19) | copy-start | bytes 1540
  99.5 11.0 %copy-start = (bf16[128,2048]{1,0:T(8,128)(2,1)S(1)}, bf16[128,2048]{1,0:T(8,128)(2,1)}, u32[]{:S(2)}) copy-start(bf16[128,2048]{1,0:T(8,128)(2,1)} %param.14) | copy-start | bytes 1572868
  100.3 13.3 %copy-start.1 = (f32[2048]{0:T(1024)S(1)}, f32[2048]{0:T(1024)}, u32[]{:S(2)}) copy-start(f32[2048]{0:T(1024)} %param.21) | copy-start | bytes 24580
  114.6 128.6 %all-gather.11.cloned.1.call-start = ((), (), s32[]{:S(2)}) async-start(), calls=%async_computation.5 | async-start | bytes 4718592 | tf_op jit(solution)/shard_map/all_gather | solution.py:107
  115.3 200.9 %all-gather.9.cloned.1.call-start = ((), (), s32[]{:S(2)}) async-start(), calls=%async_computation.4 | async-start | bytes 4718592 | tf_op jit(solution)/shard_map/all_gather | solution.py:106
  115.9 240.1 %reduce-scatter.2.cloned.1.call-start = ((), (), s32[]{:S(2)}) async-start(), calls=%async_computation.6 | async-start | bytes 2621440 | tf_op jit(solution)/shard_map/reduce_scatter | solution.py:118
Sparse Core Ops, SparseCore 0:
  32.1 62.0 all-gather.4
  114.7 51.7 all-gather.6
  168.5 74.6 all-gather.10
  245.2 70.9 all-gather.8
  326.3 29.6 reduce-scatter.1
